TPU v7x, 32 devices: a whole 2x2x4 slice. The times are simulated.
32 devices in a mesh: sp: 8 (over z, x), tp: 4 (over y, core).
Axes of the slice: x: 2, y: 2, z: 4, core: 2. Of those that a mesh axis runs over, the one named last changes fastest.
Arguments:
- resid: bfloat16 [2048, 4096], P('sp'), may hold values from -6 to 6
- queries: bfloat16 [2048, 3072], P('sp', 'tp'), may hold values from -1000 to 1000
- latent: bfloat16 [2048, 512], P('sp'), may hold values from -6 to 6
- rope_key: bfloat16 [2048, 64], P('sp'), may hold values from -6 to 6
- lat_gain: float32 [512], replicated, may hold values from 0.1 to 1.9
- kv_weight: bfloat16 [512, 4096], P(None, 'tp'), may hold values from -4 to 4
- out_gain: float32 [2048], P('tp'), may hold values from 0.1 to 1.9
- out_weight: bfloat16 [2048, 4096], P('tp'), may hold values from -0.125 to 0.125
- ffn_gain: float32 [4096], replicated, may hold values from 0.1 to 1.9
- gate_weight: bfloat16 [4096, 6144], P('sp', 'tp'), may hold values from -0.09375 to 0.09375
- up_weight: bfloat16 [4096, 6144], P('sp', 'tp'), may hold values from -0.09375 to 0.09375
- down_weight: bfloat16 [6144, 4096], P('tp', 'sp'), may hold values from -0.078125 to 0.078125
Outputs:
- result: bfloat16 [2048, 4096], P(('sp', 'tp'))
All inputs are finite; a program needn't handle non-finite values.
Results may differ from a plain program's by a relative error of at most 0.018.
Values may be sent and summed in bfloat16 or wider, within the bound.
No kernel may reach another device: no remote copies, remote signals or barrier semaphores. Data moves between devices by JAX's collectives and lax.ppermute only.
A program may use at most 192 MiB of HBM per device.

v0:
```python
import math

import jax
import jax.numpy as jnp
from jax import lax
from jax.sharding import PartitionSpec as P

HEADS = 16
NOPE = 128
ROPE = 64
VDIM = 128


EPSILON = 1e-06
THETA = 10000.0
LOWEST = -1e30


def rotate(values, places):
    half = values.shape[-1] // 2
    inverse = THETA ** (-jnp.arange(half, dtype=jnp.float32) / half)
    angle = places[..., None] * inverse
    cosine = jnp.cos(angle)
    sine = jnp.sin(angle)
    first = values[..., :half]
    second = values[..., half:]
    return jnp.concatenate(
        [first * cosine - second * sine, first * sine + second * cosine], axis=-1
    )


def norm_rows(values, gain):
    wide = values.astype(jnp.float32)
    return wide * lax.rsqrt(jnp.mean(wide * wide, axis=-1, keepdims=True) + EPSILON) * gain


def make_keys(latent_piece, rotary_piece, lat_gain, kv_weight):
    normed = norm_rows(latent_piece, lat_gain).astype(jnp.bfloat16)
    key_value = jnp.dot(normed, kv_weight, preferred_element_type=jnp.float32).astype(jnp.bfloat16)
    key_index = jnp.arange(latent_piece.shape[0], dtype=jnp.int32)
    key_rope = rotate(rotary_piece.astype(jnp.float32), key_index.astype(jnp.float32)).astype(
        jnp.bfloat16
    )
    return (key_value, key_rope)


def body(
    resid,
    queries,
    latent,
    rope_key,
    lat_gain,
    kv_weight,
    out_gain,
    out_weight,
    ffn_gain,
    gate_weight,
    up_weight,
    down_weight,
):
    rows_here = resid.shape[0]
    first_row = lax.axis_index("sp") * rows_here
    heads_here = queries.shape[1] // (NOPE + ROPE)
    query = queries.reshape(rows_here, heads_here, NOPE + ROPE)
    query_index = first_row + jnp.arange(rows_here, dtype=jnp.int32)
    query_nope = query[:, :, :NOPE]
    query_rope = rotate(
        query[:, :, NOPE:].astype(jnp.float32), query_index.astype(jnp.float32)[:, None]
    ).astype(jnp.bfloat16)
    scale = 1.0 / math.sqrt(NOPE + ROPE)

    def accumulate(state, key_value, key_rope):
        running_max, running_sum, weighted = state
        length = key_value.shape[0]
        key_value = key_value.reshape(length, heads_here, NOPE + VDIM)
        key_index = jnp.arange(length, dtype=jnp.int32)
        scores = jnp.einsum(
            "qhd,khd->hqk", query_nope, key_value[:, :, :NOPE], preferred_element_type=jnp.float32
        )
        scores = (
            scores
            + jnp.einsum("qhr,kr->hqk", query_rope, key_rope, preferred_element_type=jnp.float32)
        ) * scale
        allowed = (key_index[None, :] <= query_index[:, None])[None]
        scores = jnp.where(allowed, scores, LOWEST)
        new_max = jnp.maximum(running_max, jnp.max(scores, axis=-1))
        weights = jnp.where(allowed, jnp.exp(scores - new_max[:, :, None]), 0.0)
        running_sum = jnp.sum(weights, axis=-1)
        added = jnp.einsum(
            "hqk,khd->qhd",
            weights.astype(jnp.bfloat16),
            key_value[:, :, NOPE:],
            preferred_element_type=jnp.float32,
        )
        weighted = added
        return (new_max, running_sum, weighted)

    def unchanged(state):
        return state

    initial = (
        jnp.full((heads_here, rows_here), LOWEST, jnp.float32),
        jnp.zeros((heads_here, rows_here), jnp.float32),
        jnp.zeros((rows_here, heads_here, VDIM), jnp.float32),
    )
    pieces = (
        lax.all_gather(latent, "sp", axis=0, tiled=True),
        lax.all_gather(rope_key, "sp", axis=0, tiled=True),
    )

    def update(state):
        key_value, key_rope = make_keys(pieces[0], pieces[1], lat_gain, kv_weight)
        return accumulate(state, key_value, key_rope)

    running_max, running_sum, weighted = lax.cond(
        jnp.int32(0) < first_row + rows_here, update, unchanged, initial
    )
    attended = (weighted / jnp.transpose(running_sum)[:, :, None]).astype(jnp.bfloat16)
    attended_float = attended.reshape(rows_here, heads_here * VDIM).astype(jnp.float32)
    squares = lax.psum(jnp.sum(attended_float * attended_float, axis=1), "tp")
    normed_out = attended_float * lax.rsqrt(squares / (HEADS * VDIM) + EPSILON)[:, None] * out_gain
    normed_out = normed_out.astype(jnp.bfloat16)
    share = rows_here // lax.axis_size("tp")
    own_first = lax.axis_index("tp") * share
    attn_sum = lax.psum_scatter(
        jnp.dot(normed_out, out_weight, preferred_element_type=jnp.float32).astype(jnp.bfloat16),
        "tp",
        scatter_dimension=0,
        tiled=True,
    ).astype(jnp.float32)
    own_resid = lax.dynamic_slice_in_dim(resid, own_first, share, 0)
    middle = (own_resid.astype(jnp.float32) + attn_sum).astype(jnp.bfloat16)
    normed_mid = lax.all_gather(
        norm_rows(middle, ffn_gain).astype(jnp.bfloat16), "tp", axis=0, tiled=True
    )
    gate = jnp.dot(
        normed_mid,
        lax.all_gather(gate_weight, "sp", axis=0, tiled=True),
        preferred_element_type=jnp.float32,
    )
    upward = jnp.dot(
        normed_mid,
        lax.all_gather(up_weight, "sp", axis=0, tiled=True),
        preferred_element_type=jnp.float32,
    )
    hidden = (jax.nn.silu(gate) * upward).astype(jnp.bfloat16)
    terms = jnp.dot(
        hidden,
        lax.all_gather(down_weight, "sp", axis=1, tiled=True),
        preferred_element_type=jnp.float32,
    )
    ffn_sum = lax.psum_scatter(
        terms.astype(jnp.bfloat16), "tp", scatter_dimension=0, tiled=True
    ).astype(jnp.float32)
    return (middle.astype(jnp.float32) + ffn_sum).astype(jnp.bfloat16)


def solution(mesh):
    placed = (
        P("sp", None),
        P("sp", "tp"),
        P("sp", None),
        P("sp", None),
        P(),
        P(None, "tp"),
        P("tp"),
        P("tp", None),
        P(),
        P("sp", "tp"),
        P("sp", "tp"),
        P("tp", "sp"),
    )
    return jax.shard_map(
        body, mesh=mesh, in_specs=placed, out_specs=P(("sp", "tp"), None), check_vma=False
    )
```

profile of v0, /device:TPU:0, one launch (start us, length us, event | category | flops | bytes accessed | tf_op | source)
XLA Modules:
  0.0 732.7 jit_solution(17946913857392103547)
XLA Ops:
  6.5 0.0 all-gather.6.cloned.1.call-start
  6.5 0.7 all-gather.6.cloned.1.call-update
  7.3 0.0 reduce-scatter.3.cloned.1.call-start
  7.3 1.2 copy.20
  8.5 33.1 %all_gather.19 = bf16[2048,64]{0,1:T(8,128)(2,1)S(1)} all-gather(bf16[256,64]{0,1:T(8,128)(2,1)} %param.17), channel_id=1, replica_groups=mesh['sp'=8,'tp'=4] {'sp'}, dimensions={0}, use_global_device_ids=true | all-gather | bytes 294912 | tf_op jit(solution)/shard_map/all_gather | solution.py:108
  41.6 0.2 multiply_cosine_fusion.1
  41.9 20.0 %all-gather.6.cloned.1.call-done = bf16[2048,512]{1,0:T(8,128)(2,1)} async-done(((bf16[256,512]{1,0:T(8,128)(2,1)}), bf16[2048,512]{1,0:T(8,128)(2,1)}) %all-gather.6.cloned.1.call-update) | async-done | bytes 2097168 | tf_op jit(solution)/shard_map/all_gather | solution.py:107
  62.0 0.0 copy-start.2
  62.0 18.5 %conditional.1 = (f32[4,256]{1,0:T(4,128)S(1)}, f32[256,4,128]{0,2,1:T(8,128)S(1)}) conditional(s32[]{:T(128)} %convert_element_type.90, () %tuple.13, (s32[]{:T(128)}, s32[256]{0:T(256)S(1)}, bf16[2048,512]{1,0:T(8,128)(2,1)}, f32[512]{0:T(512)}, bf16[512,1024]{1,0:T(8,128)(2,1)}, /*index=5*/bf16[256,4,192]{0,2,1:T(8,128)(2,1)S(1)}, ...), branch_computations={%region_0.0_spmd, %region_1.5_spmd} | conditional | flops 3521842432 | bytes 78066992 | solution.py:115
  62.0 2.1 fusion.4
  64.1 6.3 convolution_convert_fusion
  70.4 0.2 copy.21
  70.6 2.9 fusion.14
  73.5 0.3 iota_compare_fusion
  74.0 1.2 fusion.28
  75.1 0.0 copy-start
  75.1 2.1 fusion.46
  77.3 0.1 copy-done
  77.3 1.7 fusion.18
  79.0 1.5 fusion.3
  80.5 0.1 multiply_reduce_fusion
  80.6 5.8 psum.7
  86.5 0.0 copy-done.2
  86.5 0.1 fusion.42
  86.6 0.0 copy-start.1
  86.6 4.8 convolution_convert_fusion.2
  91.4 0.0 reduce-scatter.3.cloned.1.call-update
  91.5 0.0 all-gather.8.cloned.1.call-start
  91.5 30.1 %reduce-scatter.3.cloned.1.call-done = bf16[64,4096]{1,0:T(8,128)(2,1)} async-done(((bf16[256,4096]{1,0:T(8,128)(2,1)}), bf16[64,4096]{1,0:T(8,128)(2,1)}) %reduce-scatter.3.cloned.1.call-update) | async-done | bytes 524304 | tf_op jit(solution)/shard_map/reduce_scatter | solution.py:125
  121.7 1.5 fusion.37
  123.2 0.0 copy-done.1
  123.2 1.0 fusion.39
  124.1 0.0 all-gather.8.cloned.1.call-update
  124.2 0.0 all-gather.10.cloned.1.call-start
  124.2 0.5 all-gather.10.cloned.1.call-update
  124.8 0.0 all-gather.12.cloned.1.call-start
  124.8 0.5 all-gather.12.cloned.1.call-update
  125.3 0.0 all-gather.14.cloned.1.call-start
  125.4 0.5 all-gather.14.cloned.1.call-update
  125.9 0.0 reduce-scatter.5.cloned.1.call-start
  126.0 20.9 %all-gather.8.cloned.1.call-done = bf16[256,4096]{1,0:T(8,128)(2,1)} async-done(((bf16[64,4096]{1,0:T(8,128)(2,1)}), bf16[256,4096]{1,0:T(8,128)(2,1)}) %all-gather.8.cloned.1.call-update) | async-done | bytes 2097168 | tf_op jit(solution)/shard_map/all_gather | solution.py:133
  146.9 0.0 copy-start.3
  146.9 178.2 %all-gather.10.cloned.1.call-done = bf16[4096,1536]{1,0:T(8,128)(2,1)} async-done(((bf16[512,1536]{1,0:T(8,128)(2,1)}), bf16[4096,1536]{1,0:T(8,128)(2,1)}) %all-gather.10.cloned.1.call-update) | async-done | bytes 12582928 | tf_op jit(solution)/shard_map/all_gather | solution.py:138
  325.1 9.7 %fusion.47 = f32[256,1536]{1,0:T(8,128)} fusion(bf16[256,4096]{1,0:T(8,128)(2,1)} %all-gather.8.cloned.1.call-done, bf16[4096,1536]{1,0:T(8,128)(2,1)} %all-gather.10.cloned.1.call-done), kind=kOutput, calls=%fused_computation.74 | convolution fusion | flops 3221225472 | bytes 16252928 | tf_op jit(solution)/shard_map/dot_general | solution.py:136
  334.8 166.6 %all-gather.12.cloned.1.call-done = bf16[4096,1536]{1,0:T(8,128)(2,1)} async-done(((bf16[512,1536]{1,0:T(8,128)(2,1)}), bf16[4096,1536]{1,0:T(8,128)(2,1)}) %all-gather.12.cloned.1.call-update) | async-done | bytes 12582928 | tf_op jit(solution)/shard_map/all_gather | solution.py:143
  501.4 176.2 %all-gather.14.cloned.1.call-done = bf16[1536,4096]{1,0:T(8,128)(2,1)} async-done(((bf16[1536,512]{1,0:T(8,128)(2,1)}), bf16[1536,4096]{1,0:T(8,128)(2,1)}) %all-gather.14.cloned.1.call-update) | async-done | bytes 12582928 | tf_op jit(solution)/shard_map/all_gather | solution.py:149
  677.6 0.0 copy-done.3
  677.6 16.7 %convolution_convert_fusion.1 = bf16[256,4096]{1,0:T(8,128)(2,1)} fusion(bf16[1536,4096]{1,0:T(8,128)(2,1)} %all-gather.14.cloned.1.call-done, bf16[256,4096]{1,0:T(8,128)(2,1)S(1)} %copy-done.3, bf16[4096,1536]{1,0:T(8,128)(2,1)} %all-gather.12.cloned.1.call-done, f32[256,1536]{1,0:T(8,128)} %fusion.47), kind=kOutput, calls=%fused_computation.44 | convolution fusion | flops 6445858816 | bytes 30932992 | tf_op jit(solution)/shard_map/dot_general | solution.py:147
  694.4 0.0 reduce-scatter.5.cloned.1.call-update
  694.4 29.5 %reduce-scatter.5.cloned.1.call-done = bf16[64,4096]{1,0:T(8,128)(2,1)} async-done(((bf16[256,4096]{1,0:T(8,128)(2,1)}), bf16[64,4096]{1,0:T(8,128)(2,1)}) %reduce-scatter.5.cloned.1.call-update) | async-done | bytes 524304 | tf_op jit(solution)/shard_map/reduce_scatter | solution.py:152
  723.9 2.0 fusion.40
  (14 shorter events, 0.2 us)
Async XLA Ops:
  6.5 55.4 %all-gather.6.cloned.1.call-start = ((), (), s32[]{:S(2)}) async-start(), calls=%async_computation.2 | async-start | bytes 2359296 | tf_op jit(solution)/shard_map/all_gather | solution.py:107
  7.3 114.4 %reduce-scatter.3.cloned.1.call-start = ((), (), s32[]{:S(2)}) async-start(), calls=%async_computation.3 | async-start | bytes 2621440 | tf_op jit(solution)/shard_map/reduce_scatter | solution.py:125
  62.0 24.5 %copy-start.2 = (f32[512]{0:T(512)S(1)}, f32[512]{0:T(512)}, u32[]{:S(2)}) copy-start(f32[512]{0:T(512)} %param.20) | copy-start | bytes 6148
  75.1 2.2 copy-start
  86.6 36.5 %copy-start.1 = (f32[4096]{0:T(1024)S(1)}, f32[4096]{0:T(1024)}, u32[]{:S(2)}) copy-start(f32[4096]{0:T(1024)} %param.22) | copy-start | bytes 49156
  91.5 55.4 %all-gather.8.cloned.1.call-start = ((), (), s32[]{:S(2)}) async-start(), calls=%async_computation.4 | async-start | bytes 2621440 | tf_op jit(solution)/shard_map/all_gather | solution.py:133
  124.2 200.9 %all-gather.10.cloned.1.call-start = ((), (), s32[]{:S(2)}) async-start(), calls=%async_computation.5 | async-start | bytes 14155776 | tf_op jit(solution)/shard_map/all_gather | solution.py:138
  124.8 376.7 %all-gather.12.cloned.1.call-start = ((), (), s32[]{:S(2)}) async-start(), calls=%async_computation.6 | async-start | bytes 14155776 | tf_op jit(solution)/shard_map/all_gather | solution.py:143
  125.3 552.3 %all-gather.14.cloned.1.call-start = ((), (), s32[]{:S(2)}) async-start(), calls=%async_computation.7 | async-start | bytes 14155776 | tf_op jit(solution)/shard_map/all_gather | solution.py:149
  125.9 598.0 %reduce-scatter.5.cloned.1.call-start = ((), (), s32[]{:S(2)}) async-start(), calls=%async_computation.8 | async-start | bytes 2621440 | tf_op jit(solution)/shard_map/reduce_scatter | solution.py:152
  146.9 530.8 %copy-start.3 = (bf16[256,4096]{1,0:T(8,128)(2,1)S(1)}, bf16[256,4096]{1,0:T(8,128)(2,1)}, u32[]{:S(2)}) copy-start(bf16[256,4096]{1,0:T(8,128)(2,1)} %all-gather.8.cloned.1.call-done) | copy-start | bytes 6291460
Sparse Core Ops, SparseCore 0:
  9.5 52.4 all-gather.5
  91.6 30.0 reduce-scatter.2
  124.3 22.5 all-gather.7
  148.9 176.0 all-gather.9
  327.1 174.2 all-gather.11
  503.3 174.2 all-gather.13
  694.5 29.3 reduce-scatter.4
where the time goes:
time: 733 us
  waiting for transfers between devices  624 us (85%)
  matrix products  44.3 us (6%)
  blocking collectives  39 us (5%)
  between operations  13.6 us (2%)
  other arithmetic  10.1 us (1%)
    all_gather x1, waiting for transfers between devices, body(): lax.all_gather(gate_weight, 'sp', axis=0, tiled=True)  178 us
    all_gather x1, waiting for transfers between devices, body(): lax.all_gather(down_weight, 'sp', axis=1, tiled=True)  176 us
    all_gather x1, waiting for transfers between devices, body(): lax.all_gather(up_weight, 'sp', axis=0, tiled=True)  167 us
    all_gather x1, blocking collectives, body(): lax.all_gather(rope_key, 'sp', axis=0, tiled=True)  33.1 us
    reduce_scatter x1, waiting for transfers between devices, body(): lax.psum_scatter(jnp.dot(normed_out, out_weight, preferred_element_type=j...  30.1 us
    reduce_scatter x1, waiting for transfers between devices, body(): lax.psum_scatter(terms.astype(jnp.bfloat16), 'tp', scatter_dimension=0, t...  29.5 us
    all_gather x1, waiting for transfers between devices, body(): lax.all_gather(norm_rows(middle, ffn_gain).astype(jnp.bfloat16), 'tp', ax...  20.9 us
    all_gather x1, waiting for transfers between devices, body(): lax.all_gather(latent, 'sp', axis=0, tiled=True)  20 us
  transfers between devices with their start and end apart: 7, of which 7 were waited for; matrix products, arithmetic and copies ran while one was open for 2% of the time, Pallas kernels for 0%

commit v1 on v0

v1 whole, which is shorter than its diff:
```python
import math

import jax
import jax.numpy as jnp
from jax import lax
from jax.sharding import PartitionSpec as P

HEADS = 16
NOPE = 128
ROPE = 64
VDIM = 128


EPSILON = 1e-06
THETA = 10000.0
LOWEST = -1e30


def rotate(values, places):
    half = values.shape[-1] // 2
    inverse = THETA ** (-jnp.arange(half, dtype=jnp.float32) / half)
    angle = places[..., None] * inverse
    cosine = jnp.cos(angle)
    sine = jnp.sin(angle)
    first = values[..., :half]
    second = values[..., half:]
    return jnp.concatenate(
        [first * cosine - second * sine, first * sine + second * cosine], axis=-1
    )


def norm_rows(values, gain):
    wide = values.astype(jnp.float32)
    return wide * lax.rsqrt(jnp.mean(wide * wide, axis=-1, keepdims=True) + EPSILON) * gain


def make_keys(latent_piece, rotary_piece, lat_gain, kv_weight):
    normed = norm_rows(latent_piece, lat_gain).astype(jnp.bfloat16)
    key_value = jnp.dot(normed, kv_weight, preferred_element_type=jnp.float32).astype(jnp.bfloat16)
    key_index = jnp.arange(latent_piece.shape[0], dtype=jnp.int32)
    key_rope = rotate(rotary_piece.astype(jnp.float32), key_index.astype(jnp.float32)).astype(
        jnp.bfloat16
    )
    return (key_value, key_rope)


def make_body(n_sp, n_tp):
    inner = 2 if n_sp % 2 == 0 else 1
    outer = n_sp // inner

    def shift(value, step):
        perm = [
            (o * inner + i, ((o + step) % outer) * inner + i)
            for o in range(outer)
            for i in range(inner)
        ]
        return lax.ppermute(value, "sp", perm)

    def with_partner(value, axis):
        if inner == 1:
            return value
        perm = [(o * inner + i, o * inner + 1 - i) for o in range(outer) for i in range(inner)]
        return jnp.concatenate([value, lax.ppermute(value, "sp", perm)], axis=axis)

    def own_first(value, place, axis):
        if inner == 1:
            return value
        return jnp.where(place == 0, value, jnp.flip(value, axis=axis))

    def body(
        resid,
        queries,
        latent,
        rope_key,
        lat_gain,
        kv_weight,
        out_gain,
        out_weight,
        ffn_gain,
        gate_weight,
        up_weight,
        down_weight,
    ):
        rows_here, width = resid.shape
        share = rows_here // n_tp
        sp_index = lax.axis_index("sp")
        tp_index = lax.axis_index("tp")
        first_row = sp_index * rows_here
        own_row = tp_index * share
        outer_index = sp_index // inner
        inner_index = sp_index % inner
        heads_here = queries.shape[1] // (NOPE + ROPE)
        rank = latent.shape[1]

        both = jnp.concatenate([latent, rope_key], axis=1)
        both = lax.all_gather(
            lax.dynamic_slice_in_dim(both, own_row, share, 0), ("sp", "tp"), axis=0, tiled=True
        )
        gate_up = jnp.concatenate(
            [with_partner(gate_weight, 0), with_partner(up_weight, 0)], axis=1
        )
        down = with_partner(down_weight, 1)

        query = queries.reshape(rows_here, heads_here, NOPE + ROPE)
        query_index = first_row + jnp.arange(rows_here, dtype=jnp.int32)
        query_nope = query[:, :, :NOPE]
        query_rope = rotate(
            query[:, :, NOPE:].astype(jnp.float32), query_index.astype(jnp.float32)[:, None]
        ).astype(jnp.bfloat16)
        scale = 1.0 / math.sqrt(NOPE + ROPE)
        key_value, key_rope = make_keys(both[:, :rank], both[:, rank:], lat_gain, kv_weight)
        length = key_value.shape[0]
        key_value = key_value.reshape(length, heads_here, NOPE + VDIM)
        key_index = jnp.arange(length, dtype=jnp.int32)
        scores = jnp.einsum(
            "qhd,khd->hqk", query_nope, key_value[:, :, :NOPE], preferred_element_type=jnp.float32
        )
        scores = (
            scores
            + jnp.einsum("qhr,kr->hqk", query_rope, key_rope, preferred_element_type=jnp.float32)
        ) * scale
        allowed = (key_index[None, :] <= query_index[:, None])[None]
        scores = jnp.where(allowed, scores, LOWEST)
        highest = jnp.max(scores, axis=-1)
        weights = jnp.where(allowed, jnp.exp(scores - highest[:, :, None]), 0.0)
        totals = jnp.sum(weights, axis=-1)
        weighted = jnp.einsum(
            "hqk,khd->qhd",
            weights.astype(jnp.bfloat16),
            key_value[:, :, NOPE:],
            preferred_element_type=jnp.float32,
        )
        attended = (weighted / jnp.transpose(totals)[:, :, None]).astype(jnp.bfloat16)
        attended_float = attended.reshape(rows_here, heads_here * VDIM).astype(jnp.float32)
        squares = lax.psum(jnp.sum(attended_float * attended_float, axis=1), "tp")
        normed_out = (
            attended_float * lax.rsqrt(squares / (HEADS * VDIM) + EPSILON)[:, None] * out_gain
        )
        normed_out = normed_out.astype(jnp.bfloat16)
        attn_sum = lax.psum_scatter(
            jnp.dot(normed_out, out_weight, preferred_element_type=jnp.float32).astype(
                jnp.bfloat16
            ),
            "tp",
            scatter_dimension=0,
            tiled=True,
        ).astype(jnp.float32)
        own_resid = lax.dynamic_slice_in_dim(resid, own_row, share, 0)
        middle = (own_resid.astype(jnp.float32) + attn_sum).astype(jnp.bfloat16)
        normed = norm_rows(middle, ffn_gain).astype(jnp.bfloat16)

        block = width // n_sp
        normed = own_first(normed.reshape(share, outer, inner, block), inner_index, 2)
        normed = normed.reshape(share, outer, inner * block)
        pieces = [
            shift(
                lax.dynamic_index_in_dim(normed, (outer_index + k) % outer, 1, keepdims=False), k
            )
            if k
            else lax.dynamic_index_in_dim(normed, outer_index, 1, keepdims=False)
            for k in range(outer)
        ]
        rows = lax.all_gather(jnp.stack(pieces), "tp", axis=1, tiled=True)
        units = gate_weight.shape[1]
        arrived = []
        for k in range(1, outer):
            part = jnp.dot(rows[k], gate_up, preferred_element_type=jnp.float32)
            arrived.append(shift(part.astype(jnp.bfloat16), -k))
        total = jnp.dot(rows[0], gate_up, preferred_element_type=jnp.float32)
        for part in arrived:
            total = total + part.astype(jnp.float32)
        hidden = (jax.nn.silu(total[:, :units]) * total[:, units:]).astype(jnp.bfloat16)
        terms = [
            jnp.dot(
                shift(hidden, k) if k else hidden, down, preferred_element_type=jnp.float32
            ).astype(jnp.bfloat16)
            for k in range(outer)
        ]
        summed = lax.psum_scatter(jnp.stack(terms), "tp", scatter_dimension=1, tiled=True)
        back = [shift(summed[k], -k) if k else summed[0] for k in range(outer)]
        turned = lax.dynamic_slice_in_dim(jnp.stack(back + back), outer - outer_index, outer, 0)
        ffn_sum = jnp.transpose(turned, (1, 0, 2)).reshape(share, outer, inner, block)
        ffn_sum = own_first(ffn_sum, inner_index, 2).reshape(share, width).astype(jnp.float32)
        return (middle.astype(jnp.float32) + ffn_sum).astype(jnp.bfloat16)

    return body


def solution(mesh):
    placed = (
        P("sp", None),
        P("sp", "tp"),
        P("sp", None),
        P("sp", None),
        P(),
        P(None, "tp"),
        P("tp"),
        P("tp", None),
        P(),
        P("sp", "tp"),
        P("sp", "tp"),
        P("tp", "sp"),
    )
    return jax.shard_map(
        make_body(mesh.shape["sp"], mesh.shape["tp"]),
        mesh=mesh,
        in_specs=placed,
        out_specs=P(("sp", "tp"), None),
        check_vma=False,
    )
```

time: 733 us -> 522 us (0.71)
  waiting for transfers between devices: 624 us -> 393 us
  blocking collectives: 39 us -> 6.97 us
  starting transfers between devices: 0.24 us -> 23.2 us
  local copies, waits for them, and re-layouts: 1.44 us -> 16.4 us
  matrix products: 44.3 us -> 55.9 us
    all_gather x5 -> x2, waiting for transfers between devices: 562 us -> 59.7 us  [the longest x1 59.7 us: body(): lax.all_gather(lax.dynamic_slice_in_dim(both, own_row, share, 0), ('sp',...]
    ppermute x0 -> x15, waiting for transfers between devices: none -> 258 us  [the longest x12 189 us: shift(): return lax.ppermute(value, 'sp', perm)]
    all_gather x1 -> x0, blocking collectives: 33.1 us -> none  [body(): lax.all_gather(rope_key, 'sp', axis=0, tiled=True)]
    ppermute x0 -> x15, starting transfers between devices: none -> 22.9 us  [the longest x12 19.2 us: shift(): return lax.ppermute(value, 'sp', perm)]
    reduce_scatter x1, waiting for transfers between devices: 29.5 us -> 45.6 us  [body(): lax.psum_scatter(jnp.stack(terms), 'tp', scatter_dimension=1, tiled=True)]
    sub x0 -> x1, matrix products: none -> 7.96 us  [body(): weights = jnp.where(allowed, jnp.exp(scores - highest[:, :, None]), 0.0)]
    dot_general x5 -> x10, matrix products: 33.2 us -> 39 us  [the longest x1 15.2 us: body(): total = jnp.dot(rows[0], gate_up, preferred_element_type=jnp.float32)]
  transfers between devices with their start and end apart: 7 -> 19, of which waited for: 7 -> 13; matrix products, arithmetic and copies ran while one was open for 2% -> 5% of each run, Pallas kernels for 0% -> 0%
where the time goes in v1:
time: 522 us
  waiting for transfers between devices  393 us (75%)
  matrix products  55.9 us (11%)
  starting transfers between devices  23.2 us (4%)
  local copies, waits for them, and re-layouts  16.4 us (3%)
  between operations  13.7 us (3%)
  other arithmetic  12.8 us (2%)
  blocking collectives  6.97 us (1%)
    ppermute x12, waiting for transfers between devices, shift(): return lax.ppermute(value, 'sp', perm)  189 us
    ppermute x3, waiting for transfers between devices, with_partner(): return jnp.concatenate([value, lax.ppermute(value, 'sp', perm)], axis=axis)  68.2 us
    all_gather x1, waiting for transfers between devices, body(): lax.all_gather(lax.dynamic_slice_in_dim(both, own_row, share, 0), ('sp',...  59.7 us
    reduce_scatter x1, waiting for transfers between devices, body(): lax.psum_scatter(jnp.stack(terms), 'tp', scatter_dimension=1, tiled=True)  45.6 us
    reduce_scatter x1, waiting for transfers between devices, body(): lax.psum_scatter(jnp.dot(normed_out, out_weight, preferred_element_type=j...  29.6 us
    ppermute x12, starting transfers between devices, shift(): return lax.ppermute(value, 'sp', perm)  19.2 us
    dot_general x1, matrix products, body(): total = jnp.dot(rows[0], gate_up, preferred_element_type=jnp.float32)  15.2 us
    dot_general x3, matrix products, body(): part = jnp.dot(rows[k], gate_up, preferred_element_type=jnp.float32)  11.8 us
  transfers between devices with their start and end apart: 19, of which 13 were waited for; matrix products, arithmetic and copies ran while one was open for 5% of the time, Pallas kernels for 0%

profile of v1, /device:TPU:0, one launch (start us, length us, event | category | flops | bytes accessed | tf_op | source)
XLA Modules:
  0.0 521.5 jit_solution(13246865164181568366)
XLA Ops:
  6.5 1.0 copy.27
  7.5 1.5 fusion.63
  9.1 1.2 copy.29
  10.6 0.3 iota_compare_fusion
  10.9 59.7 %all-gather.3.cloned.1.call-done = bf16[2048,576]{1,0:T(8,128)(2,1)} async-done(((bf16[64,576]{1,0:T(8,128)(2,1)}), bf16[2048,576]{1,0:T(8,128)(2,1)}) %all-gather.3.cloned.1.call-update) | async-done | bytes 2359312 | tf_op jit(solution)/shard_map/all_gather | solution.py:96
  70.6 2.1 fusion.3
  72.8 4.1 convolution_convert_fusion.4
  76.9 4.6 fusion.11
  81.7 1.2 fusion.54
  82.9 8.0 %fusion.66 = (f32[4,256]{1,0:T(4,128)S(1)}, bf16[4,256,2048]{1,2,0:T(8,128)(2,1)}) fusion(pred[256,2048]{0,1:T(8,128)(4,1)S(1)} %iota_compare_fusion, f32[4,2048,256]{2,1,0:T(8,128)} %fusion.11, bf16[2048,32]{0,1:T(8,128)(2,1)S(1)} %get-tuple-element.8, bf16[2048,32]{0,1:T(8,128)(2,1)S(1)} %get-tuple-element.7, ...), kind=kOutput, calls=%fused_computation.118 | convolution fusion | flops 283904000 | bytes 13504512 | tf_op jit(solution)/shard_map/sub | solution.py:125
  90.8 3.6 multiply_reduce_fusion
  94.4 7.0 %psum.7 = f32[256]{0:T(256)S(1)} all-reduce(f32[256]{0:T(256)S(1)} %get-tuple-element.23), channel_id=1, replica_groups=mesh['sp'=8,'tp'=4] {'tp'}, use_global_device_ids=true, to_apply=%region_4.5 | all-reduce | flops 256 | bytes 2048 | tf_op jit(solution)/shard_map/psum | solution.py:135
  101.5 4.8 convolution_convert_fusion
  106.4 0.2 all-gather.5.cloned.1.call-start
  106.7 29.6 %reduce-scatter.3.cloned.1.call-done = bf16[64,4096]{1,0:T(8,128)(2,1)} async-done(((bf16[256,4096]{1,0:T(8,128)(2,1)}), bf16[64,4096]{1,0:T(8,128)(2,1)}) %reduce-scatter.3.cloned.1.call-update) | async-done | bytes 524304 | tf_op jit(solution)/shard_map/reduce_scatter | solution.py:140
  136.3 1.5 fusion.42
  138.0 0.4 reshape.148
  138.4 2.8 rev.7
  141.2 0.3 reshape.154
  141.6 1.1 constant_dynamic-slice_fusion.3
  142.7 1.5 collective-permute-start
  144.3 2.5 collective-permute-start.1
  146.8 1.5 collective-permute-start.2
  148.4 2.7 collective-permute-done
  151.0 4.3 collective-permute-done.1
  155.4 0.9 pad_maximum_fusion.1
  156.3 1.5 collective-permute-start.3
  157.9 0.5 collective-permute-start.4
  158.4 35.6 %collective-permute-done.3 = bf16[512,1536]{1,0:T(8,128)(2,1)} collective-permute-done((bf16[512,1536]{1,0:T(8,128)(2,1)}, bf16[512,1536]{1,0:T(8,128)(2,1)}, u32[]{:S(2)}, u32[]{:S(2)}) %collective-permute-start.3) | collective-permute-done | bytes 1572896 | tf_op jit(solution)/shard_map/ppermute | solution.py:63
  193.9 32.7 %collective-permute-done.4 = bf16[512,1536]{1,0:T(8,128)(2,1)} collective-permute-done((bf16[512,1536]{1,0:T(8,128)(2,1)S(1)}, bf16[512,1536]{1,0:T(8,128)(2,1)}, u32[]{:S(2)}, u32[]{:S(2)}) %collective-permute-start.4) | collective-permute-done | bytes 1572896 | tf_op jit(solution)/shard_map/ppermute | solution.py:63
  226.6 4.4 convolution_convert_fusion.3
  231.1 3.1 collective-permute-start.5
  234.2 3.7 convolution_convert_fusion.2
  237.9 1.8 collective-permute-start.6
  239.7 3.7 convolution_convert_fusion.1
  243.5 1.5 collective-permute-start.8
  245.0 24.1 %collective-permute-done.5 = bf16[256,3072]{1,0:T(8,128)(2,1)S(1)} collective-permute-done((bf16[256,3072]{1,0:T(8,128)(2,1)S(1)}, bf16[256,3072]{1,0:T(8,128)(2,1)S(1)}, u32[]{:S(2)}, u32[]{:S(2)}) %collective-permute-start.5) | collective-permute-done | bytes 1572896 | tf_op jit(solution)/shard_map/ppermute | solution.py:57
  269.1 101.4 %collective-permute-done.6 = bf16[256,3072]{1,0:T(8,128)(2,1)S(1)} collective-permute-done((bf16[256,3072]{1,0:T(8,128)(2,1)S(1)}, bf16[256,3072]{1,0:T(8,128)(2,1)S(1)}, u32[]{:S(2)}, u32[]{:S(2)}) %collective-permute-start.6) | collective-permute-done | bytes 1572896 | tf_op jit(solution)/shard_map/ppermute | solution.py:57
  370.5 15.2 %fusion.9 = f32[256,3072]{1,0:T(8,128)S(1)} fusion(bf16[256,3072]{1,0:T(8,128)(2,1)S(1)} %collective-permute-done.7, bf16[256,3072]{1,0:T(8,128)(2,1)S(1)} %collective-permute-done.6, bf16[256,3072]{1,0:T(8,128)(2,1)S(1)} %collective-permute-done.5, bf16[4,256,1024]{2,1,0:T(8,128)(2,1)S(1)} %copy-done.6, bf16[512,1536]{1,0:T(8,128)(2,1)} %collective-permute-done.4, ...), kind=kOutput, calls=%fused_computation.16 | convolution fusion | flops 1640497152 | bytes 14680064 | tf_op jit(solution)/shard_map/dot_general | solution.py:169
  385.7 0.5 fusion.17
  386.1 0.3 collective-permute-start.9
  386.4 0.2 constant_dynamic-update-slice_fusion.1
  386.8 0.2 constant_dynamic-update-slice_fusion
  387.0 3.9 collective-permute-start.11
  390.9 1.0 fusion.18
  391.8 16.9 %collective-permute-done.9 = bf16[256,1536]{1,0:T(8,128)(2,1)S(1)} collective-permute-done((bf16[256,1536]{1,0:T(8,128)(2,1)S(1)}, bf16[256,1536]{1,0:T(8,128)(2,1)S(1)}, u32[]{:S(2)}, u32[]{:S(2)}) %collective-permute-start.9) | collective-permute-done | bytes 786464 | tf_op jit(solution)/shard_map/ppermute | solution.py:57
  408.7 1.0 fusion.19
  409.7 30.1 %collective-permute-done.10 = bf16[256,1536]{1,0:T(8,128)(2,1)S(1)} collective-permute-done((bf16[256,1536]{1,0:T(8,128)(2,1)S(1)}, bf16[256,1536]{1,0:T(8,128)(2,1)S(1)}, u32[]{:S(2)}, u32[]{:S(2)}) %collective-permute-start.10) | collective-permute-done | bytes 786464 | tf_op jit(solution)/shard_map/ppermute | solution.py:57
  439.8 1.0 fusion.20
  440.8 1.0 fusion.21
  441.8 1.6 pad_maximum_fusion
  443.4 45.6 %reduce-scatter.5.cloned.1.call-done = bf16[4,64,1024]{2,1,0:T(8,128)(2,1)} async-done(((bf16[4,256,1024]{2,1,0:T(8,128)(2,1)}), bf16[4,64,1024]{2,1,0:T(8,128)(2,1)}) %reduce-scatter.5.cloned.1.call-update) | async-done | bytes 524304 | tf_op jit(solution)/shard_map/reduce_scatter | solution.py:179
  489.0 1.1 slice_bitcast_fusion.8
  490.2 3.4 collective-permute-start.12
  493.6 1.1 collective-permute-start.14
  494.7 2.8 collective-permute-done.12
  497.4 7.2 %collective-permute-done.13 = bf16[64,1024]{1,0:T(8,128)(2,1)S(1)} collective-permute-done((bf16[64,1024]{1,0:T(8,128)(2,1)S(1)}, bf16[64,1024]{1,0:T(8,128)(2,1)S(1)}, u32[]{:S(2)}, u32[]{:S(2)}) %collective-permute-start.13) | collective-permute-done | bytes 131104 | tf_op jit(solution)/shard_map/ppermute | solution.py:57
  504.7 0.9 slice_dynamic-update-slice_fusion.1
  505.7 0.4 reshape.150
  506.1 0.4 copy.35
  506.5 4.0 rev.8
  510.5 0.5 fusion.46
  511.0 1.9 reshape.152
  512.9 2.1 fusion.45
  (63 shorter events, 1.6 us)
Async XLA Ops:
  6.5 66.2 %copy-start = (bf16[512,1024]{1,0:T(8,128)(2,1)S(1)}, bf16[512,1024]{1,0:T(8,128)(2,1)}, u32[]{:S(2)}) copy-start(bf16[512,1024]{1,0:T(8,128)(2,1)} %param.17) | copy-start | bytes 3145732
  6.5 66.2 %copy-start.9 = (f32[512]{0:T(512)S(1)}, f32[512]{0:T(512)}, u32[]{:S(2)}) copy-start(f32[512]{0:T(512)} %param.16) | copy-start | bytes 6148
  6.5 64.1 %all-gather.3.cloned.1.call-start = ((), (), s32[]{:S(2)}) async-start(), calls=%async_computation.2 | async-start | bytes 2703360 | tf_op jit(solution)/shard_map/all_gather | solution.py:96
  9.0 127.3 %reduce-scatter.3.cloned.1.call-start = ((), (), s32[]{:S(2)}) async-start(), calls=%async_computation.3 | async-start | bytes 2621440 | tf_op jit(solution)/shard_map/reduce_scatter | solution.py:140
  76.9 4.6 copy-start.3
  76.9 4.6 slice-start
  90.8 10.6 %copy-start.5 = (f32[512]{0:T(512)S(1)}, f32[512]{0:T(512)}, u32[]{:S(2)}) copy-start(f32[512]{0:T(512)} %param.18) | copy-start | bytes 6148
  106.4 31.4 %copy-start.4 = (f32[4096]{0:T(1024)S(1)}, f32[4096]{0:T(1024)}, u32[]{:S(2)}) copy-start(f32[4096]{0:T(1024)} %param.20) | copy-start | bytes 49156
  106.4 120.2 %all-gather.5.cloned.1.call-start = ((), (), s32[]{:S(2)}) async-start(), calls=%async_computation.4 | async-start | bytes 2621440 | tf_op jit(solution)/shard_map/all_gather | solution.py:163
  141.2 16.6 %copy-start.7 = (bf16[512,1536]{1,0:T(8,128)(2,1)S(1)}, bf16[512,1536]{1,0:T(8,128)(2,1)}, u32[]{:S(2)}) copy-start(bf16[512,1536]{1,0:T(8,128)(2,1)} %param.22) | copy-start | bytes 4718596
  142.7 8.3 %collective-permute-start = (bf16[64,1024]{1,0:T(8,128)(2,1)S(1)}, bf16[64,1024]{1,0:T(8,128)(2,1)S(1)}, u32[]{:S(2)}, u32[]{:S(2)}) collective-permute-start(bf16[64,1024]{1,0:T(8,128)(2,1)S(1)} %bitcast.111), channel_id=1, source_target_pairs={{0,8},{4,12},{8,16},{12,20},{16,24},{20,28},{24,0},{28,4},{1,9},{5... | collective-permute-start | bytes 393224 | tf_op jit(solution)/shard_map/ppermute | solution.py:57
  144.3 11.1 %collective-permute-start.1 = (bf16[64,1024]{1,0:T(8,128)(2,1)S(1)}, bf16[64,1024]{1,0:T(8,128)(2,1)S(1)}, u32[]{:S(2)}, u32[]{:S(2)}) collective-permute-start(bf16[64,1024]{1,0:T(8,128)(2,1)S(1)} %bitcast.112), channel_id=1, source_target_pairs={{0,16},{4,20},{8,24},{12,28},{16,0},{20,4},{24,8},{28,12},{1,17},{... | collective-permute-start | bytes 393224 | tf_op jit(solution)/shard_map/ppermute | solution.py:57
  146.8 8.5 %collective-permute-start.2 = (bf16[64,1024]{1,0:T(8,128)(2,1)S(1)}, bf16[64,1024]{1,0:T(8,128)(2,1)S(1)}, u32[]{:S(2)}, u32[]{:S(2)}) collective-permute-start(bf16[64,1024]{1,0:T(8,128)(2,1)S(1)} %bitcast.113), channel_id=1, source_target_pairs={{0,24},{4,28},{8,0},{12,4},{16,8},{20,12},{24,16},{28,20},{1,25},{... | collective-permute-start | bytes 393224 | tf_op jit(solution)/shard_map/ppermute | solution.py:57
  156.3 332.8 %reduce-scatter.5.cloned.1.call-start = ((), (), s32[]{:S(2)}) async-start(), calls=%async_computation.5 | async-start | bytes 2621440 | tf_op jit(solution)/shard_map/reduce_scatter | solution.py:179
  156.3 37.6 %collective-permute-start.3 = (bf16[512,1536]{1,0:T(8,128)(2,1)}, bf16[512,1536]{1,0:T(8,128)(2,1)}, u32[]{:S(2)}, u32[]{:S(2)}) collective-permute-start(bf16[512,1536]{1,0:T(8,128)(2,1)} %param.21), channel_id=1, source_target_pairs={{0,4},{4,0},{8,12},{12,8},{16,20},{20,16},{24,28},{28,24},{1,5},{5... | collective-permute-start | bytes 4718600 | tf_op jit(solution)/shard_map/ppermute | solution.py:63
  157.9 68.8 %collective-permute-start.4 = (bf16[512,1536]{1,0:T(8,128)(2,1)S(1)}, bf16[512,1536]{1,0:T(8,128)(2,1)}, u32[]{:S(2)}, u32[]{:S(2)}) collective-permute-start(bf16[512,1536]{1,0:T(8,128)(2,1)S(1)} %copy-done.7), channel_id=1, source_target_pairs={{0,4},{4,0},{8,12},{12,8},{16,20},{20,16},{24,28},{28,24},{1,5},{5... | collective-permute-start | bytes 4718600 | tf_op jit(solution)/shard_map/ppermute | solution.py:63
  226.6 7.6 %copy-start.6 = (bf16[4,256,1024]{2,1,0:T(8,128)(2,1)S(1)}, bf16[4,256,1024]{2,1,0:T(8,128)(2,1)}, u32[]{:S(2)}) copy-start(bf16[4,256,1024]{2,1,0:T(8,128)(2,1)} %all-gather.5.cloned.1.call-done) | copy-start | bytes 6291460
  226.6 7.6 %copy-start.8 = (bf16[512,1536]{1,0:T(8,128)(2,1)S(1)}, bf16[512,1536]{1,0:T(8,128)(2,1)}, u32[]{:S(2)}) copy-start(bf16[512,1536]{1,0:T(8,128)(2,1)} %param.21) | copy-start | bytes 4718596
  231.1 38.0 %collective-permute-start.5 = (bf16[256,3072]{1,0:T(8,128)(2,1)S(1)}, bf16[256,3072]{1,0:T(8,128)(2,1)S(1)}, u32[]{:S(2)}, u32[]{:S(2)}) collective-permute-start(bf16[256,3072]{1,0:T(8,128)(2,1)S(1)} %convolution_convert_fusion.3), channel_id=1, source_target_pairs={{0,24},{4,28},{8,0},{12,4},{16,8},{20,12},{24,16},{28,20},{1,25},{... | collective-permute-start | bytes 4718600 | tf_op jit(solution)/shard_map/ppermute | solution.py:57
  237.9 5.6 %copy-start.2 = (bf16[1536,512]{1,0:T(8,128)(2,1)S(1)}, bf16[1536,512]{1,0:T(8,128)(2,1)}, u32[]{:S(2)}) copy-start(bf16[1536,512]{1,0:T(8,128)(2,1)} %param.23) | copy-start | bytes 4718596
  237.9 132.6 %collective-permute-start.6 = (bf16[256,3072]{1,0:T(8,128)(2,1)S(1)}, bf16[256,3072]{1,0:T(8,128)(2,1)S(1)}, u32[]{:S(2)}, u32[]{:S(2)}) collective-permute-start(bf16[256,3072]{1,0:T(8,128)(2,1)S(1)} %convolution_convert_fusion.2), channel_id=1, source_target_pairs={{0,16},{4,20},{8,24},{12,28},{16,0},{20,4},{24,8},{28,12},{1,17},{... | collective-permute-start | bytes 4718600 | tf_op jit(solution)/shard_map/ppermute | solution.py:57
  243.4 127.1 %collective-permute-start.7 = (bf16[256,3072]{1,0:T(8,128)(2,1)S(1)}, bf16[256,3072]{1,0:T(8,128)(2,1)S(1)}, u32[]{:S(2)}, u32[]{:S(2)}) collective-permute-start(bf16[256,3072]{1,0:T(8,128)(2,1)S(1)} %convolution_convert_fusion.1), channel_id=1, source_target_pairs={{0,8},{4,12},{8,16},{12,20},{16,24},{20,28},{24,0},{28,4},{1,9},{5... | collective-permute-start | bytes 4718600 | tf_op jit(solution)/shard_map/ppermute | solution.py:57
  243.5 143.3 %collective-permute-start.8 = (bf16[1536,512]{1,0:T(8,128)(2,1)S(1)}, bf16[1536,512]{1,0:T(8,128)(2,1)S(1)}, u32[]{:S(2)}, u32[]{:S(2)}) collective-permute-start(bf16[1536,512]{1,0:T(8,128)(2,1)S(1)} %copy-done.2), channel_id=1, source_target_pairs={{0,4},{4,0},{8,12},{12,8},{16,20},{20,16},{24,28},{28,24},{1,5},{5... | collective-permute-start | bytes 4718600 | tf_op jit(solution)/shard_map/ppermute | solution.py:63
  386.1 22.6 %collective-permute-start.9 = (bf16[256,1536]{1,0:T(8,128)(2,1)S(1)}, bf16[256,1536]{1,0:T(8,128)(2,1)S(1)}, u32[]{:S(2)}, u32[]{:S(2)}) collective-permute-start(bf16[256,1536]{1,0:T(8,128)(2,1)S(1)} %fusion.17), channel_id=1, source_target_pairs={{0,8},{4,12},{8,16},{12,20},{16,24},{20,28},{24,0},{28,4},{1,9},{5... | collective-permute-start | bytes 2359304 | tf_op jit(solution)/shard_map/ppermute | solution.py:57
  386.7 53.1 %collective-permute-start.10 = (bf16[256,1536]{1,0:T(8,128)(2,1)S(1)}, bf16[256,1536]{1,0:T(8,128)(2,1)S(1)}, u32[]{:S(2)}, u32[]{:S(2)}) collective-permute-start(bf16[256,1536]{1,0:T(8,128)(2,1)S(1)} %fusion.17), channel_id=1, source_target_pairs={{0,16},{4,20},{8,24},{12,28},{16,0},{20,4},{24,8},{28,12},{1,17},{... | collective-permute-start | bytes 2359304 | tf_op jit(solution)/shard_map/ppermute | solution.py:57
  387.0 53.8 %collective-permute-start.11 = (bf16[256,1536]{1,0:T(8,128)(2,1)S(1)}, bf16[256,1536]{1,0:T(8,128)(2,1)S(1)}, u32[]{:S(2)}, u32[]{:S(2)}) collective-permute-start(bf16[256,1536]{1,0:T(8,128)(2,1)S(1)} %fusion.17), channel_id=1, source_target_pairs={{0,24},{4,28},{8,0},{12,4},{16,8},{20,12},{24,16},{28,20},{1,25},{... | collective-permute-start | bytes 2359304 | tf_op jit(solution)/shard_map/ppermute | solution.py:57
  490.2 7.3 %collective-permute-start.12 = (bf16[64,1024]{1,0:T(8,128)(2,1)S(1)}, bf16[64,1024]{1,0:T(8,128)(2,1)S(1)}, u32[]{:S(2)}, u32[]{:S(2)}) collective-permute-start(bf16[64,1024]{1,0:T(8,128)(2,1)S(1)} %get-tuple-element.12), channel_id=1, source_target_pairs={{0,24},{4,28},{8,0},{12,4},{16,8},{20,12},{24,16},{28,20},{1,25},{... | collective-permute-start | bytes 393224 | tf_op jit(solution)/shard_map/ppermute | solution.py:57
  493.5 11.1 %collective-permute-start.13 = (bf16[64,1024]{1,0:T(8,128)(2,1)S(1)}, bf16[64,1024]{1,0:T(8,128)(2,1)S(1)}, u32[]{:S(2)}, u32[]{:S(2)}) collective-permute-start(bf16[64,1024]{1,0:T(8,128)(2,1)S(1)} %get-tuple-element.11), channel_id=1, source_target_pairs={{0,16},{4,20},{8,24},{12,28},{16,0},{20,4},{24,8},{28,12},{1,17},{... | collective-permute-start | bytes 393224 | tf_op jit(solution)/shard_map/ppermute | solution.py:57
  493.6 11.1 %collective-permute-start.14 = (bf16[64,1024]{1,0:T(8,128)(2,1)S(1)}, bf16[64,1024]{1,0:T(8,128)(2,1)S(1)}, u32[]{:S(2)}, u32[]{:S(2)}) collective-permute-start(bf16[64,1024]{1,0:T(8,128)(2,1)S(1)} %get-tuple-element.9), channel_id=1, source_target_pairs={{0,8},{4,12},{8,16},{12,20},{16,24},{20,28},{24,0},{28,4},{1,9},{5... | collective-permute-start | bytes 393224 | tf_op jit(solution)/shard_map/ppermute | solution.py:57
  506.5 8.6 %copy-start.1 = (bf16[512,1024]{1,0:T(8,128)(2,1)S(1)}, bf16[512,1024]{1,0:T(8,128)(2,1)}, u32[]{:S(2)}) copy-start(bf16[512,1024]{1,0:T(8,128)(2,1)} %param.17) | copy-start | bytes 3145732
Sparse Core Ops, SparseCore 0:
  10.2 60.3 all-gather.2
  106.5 29.7 reduce-scatter.2
  156.4 23.4 all-gather.4
  443.5 45.4 reduce-scatter.4

commit v2 on v1

--- a/solution.py
+++ b/solution.py
@@ -34,10 +34,9 @@
     return wide * lax.rsqrt(jnp.mean(wide * wide, axis=-1, keepdims=True) + EPSILON) * gain
 
 
-def make_keys(latent_piece, rotary_piece, lat_gain, kv_weight):
+def make_keys(latent_piece, rotary_piece, key_index, lat_gain, kv_weight):
     normed = norm_rows(latent_piece, lat_gain).astype(jnp.bfloat16)
     key_value = jnp.dot(normed, kv_weight, preferred_element_type=jnp.float32).astype(jnp.bfloat16)
-    key_index = jnp.arange(latent_piece.shape[0], dtype=jnp.int32)
     key_rope = rotate(rotary_piece.astype(jnp.float32), key_index.astype(jnp.float32)).astype(
         jnp.bfloat16
     )
@@ -62,10 +61,32 @@
         perm = [(o * inner + i, o * inner + 1 - i) for o in range(outer) for i in range(inner)]
         return jnp.concatenate([value, lax.ppermute(value, "sp", perm)], axis=axis)
 
-    def own_first(value, place, axis):
+    def own_first(value, place):
         if inner == 1:
             return value
-        return jnp.where(place == 0, value, jnp.flip(value, axis=axis))
+        wide = value.shape[1] // n_sp
+        swapped = [value[:, (b ^ 1) * wide : ((b ^ 1) + 1) * wide] for b in range(n_sp)]
+        return jnp.where(place == 0, value, jnp.concatenate(swapped, axis=1))
+
+    def across(value, step):
+        return lax.ppermute(value, "tp", [(t, t ^ step) for t in range(n_tp)])
+
+    def gather_tp(value):
+        tail = value.shape
+        step, axis = n_tp // 2, 0
+        while step:
+            value = jnp.stack([value, across(value, step)], axis=axis)
+            step, axis = step // 2, axis + 1
+        return value.reshape((n_tp,) + tail)
+
+    def reduce_tp(value):
+        tail = value.shape[1:]
+        step = 1
+        while step < n_tp:
+            pair = value.astype(jnp.bfloat16).reshape((value.shape[0] // 2, 2) + tail)
+            value = pair[:, 0].astype(jnp.float32) + across(pair[:, 1], step).astype(jnp.float32)
+            step *= 2
+        return value[0]
 
     def body(
         resid,
@@ -93,13 +114,23 @@
         rank = latent.shape[1]
 
         both = jnp.concatenate([latent, rope_key], axis=1)
-        both = lax.all_gather(
-            lax.dynamic_slice_in_dim(both, own_row, share, 0), ("sp", "tp"), axis=0, tiled=True
-        )
-        gate_up = jnp.concatenate(
-            [with_partner(gate_weight, 0), with_partner(up_weight, 0)], axis=1
-        )
+        both = lax.dynamic_slice_in_dim(both, own_row, share, 0)
+        around = [
+            lax.ppermute(both, "sp", [(s, (s + k) % n_sp) for s in range(n_sp)])
+            for k in range(1, n_sp)
+        ]
+        both = gather_tp(jnp.stack([both] + around)).reshape(n_tp * n_sp * share, -1)
+        owner = (sp_index - jnp.arange(n_sp, dtype=jnp.int32)) % n_sp
+        slot = tp_index ^ jnp.arange(n_tp, dtype=jnp.int32)
+        key_index = (
+            owner[None, :, None] * rows_here
+            + slot[:, None, None] * share
+            + jnp.arange(share, dtype=jnp.int32)[None, None, :]
+        ).reshape(-1)
+        gate_both = with_partner(gate_weight, 0)
+        up_both = with_partner(up_weight, 0)
         down = with_partner(down_weight, 1)
+        gate_up = jnp.concatenate([gate_both, up_both], axis=1)
 
         query = queries.reshape(rows_here, heads_here, NOPE + ROPE)
         query_index = first_row + jnp.arange(rows_here, dtype=jnp.int32)
@@ -108,10 +139,9 @@
             query[:, :, NOPE:].astype(jnp.float32), query_index.astype(jnp.float32)[:, None]
         ).astype(jnp.bfloat16)
         scale = 1.0 / math.sqrt(NOPE + ROPE)
-        key_value, key_rope = make_keys(both[:, :rank], both[:, rank:], lat_gain, kv_weight)
+        key_value, key_rope = make_keys(both[:, :rank], both[:, rank:], key_index, lat_gain, kv_weight)
         length = key_value.shape[0]
         key_value = key_value.reshape(length, heads_here, NOPE + VDIM)
-        key_index = jnp.arange(length, dtype=jnp.int32)
         scores = jnp.einsum(
             "qhd,khd->hqk", query_nope, key_value[:, :, :NOPE], preferred_element_type=jnp.float32
         )
@@ -136,37 +166,37 @@
         normed_out = (
             attended_float * lax.rsqrt(squares / (HEADS * VDIM) + EPSILON)[:, None] * out_gain
         )
-        normed_out = normed_out.astype(jnp.bfloat16)
-        attn_sum = lax.psum_scatter(
-            jnp.dot(normed_out, out_weight, preferred_element_type=jnp.float32).astype(
-                jnp.bfloat16
-            ),
-            "tp",
-            scatter_dimension=0,
-            tiled=True,
-        ).astype(jnp.float32)
+        normed_out = normed_out.astype(jnp.bfloat16).reshape(n_tp, share, heads_here * VDIM)
+        normed_out = jnp.concatenate(
+            [
+                lax.dynamic_index_in_dim(normed_out, tp_index ^ j, 0, keepdims=False)
+                for j in range(n_tp)
+            ]
+        )
+        product = jnp.dot(normed_out, out_weight, preferred_element_type=jnp.float32)
+        attn_sum = reduce_tp(product.astype(jnp.bfloat16).reshape(n_tp, share, width))
         own_resid = lax.dynamic_slice_in_dim(resid, own_row, share, 0)
         middle = (own_resid.astype(jnp.float32) + attn_sum).astype(jnp.bfloat16)
         normed = norm_rows(middle, ffn_gain).astype(jnp.bfloat16)
 
         block = width // n_sp
-        normed = own_first(normed.reshape(share, outer, inner, block), inner_index, 2)
-        normed = normed.reshape(share, outer, inner * block)
+        normed = own_first(normed, inner_index)
+        span = inner * block
         pieces = [
-            shift(
-                lax.dynamic_index_in_dim(normed, (outer_index + k) % outer, 1, keepdims=False), k
-            )
-            if k
-            else lax.dynamic_index_in_dim(normed, outer_index, 1, keepdims=False)
+            lax.dynamic_slice_in_dim(normed, (outer_index + k) % outer * span, span, 1)
             for k in range(outer)
         ]
-        rows = lax.all_gather(jnp.stack(pieces), "tp", axis=1, tiled=True)
+        pieces = [shift(piece, k) if k else piece for k, piece in enumerate(pieces)]
+        rows = gather_tp(jnp.stack(pieces))
+        rows = [rows[:, k].reshape(rows_here, span) for k in range(outer)]
         units = gate_weight.shape[1]
         arrived = []
         for k in range(1, outer):
             part = jnp.dot(rows[k], gate_up, preferred_element_type=jnp.float32)
             arrived.append(shift(part.astype(jnp.bfloat16), -k))
-        total = jnp.dot(rows[0], gate_up, preferred_element_type=jnp.float32)
+        total = lax.optimization_barrier(
+            jnp.dot(rows[0], gate_up, preferred_element_type=jnp.float32)
+        )
         for part in arrived:
             total = total + part.astype(jnp.float32)
         hidden = (jax.nn.silu(total[:, :units]) * total[:, units:]).astype(jnp.bfloat16)
@@ -176,11 +206,12 @@
             ).astype(jnp.bfloat16)
             for k in range(outer)
         ]
-        summed = lax.psum_scatter(jnp.stack(terms), "tp", scatter_dimension=1, tiled=True)
+        terms = [term.reshape(n_tp, share, span) for term in terms]
+        summed = reduce_tp(jnp.stack(terms, axis=1)).astype(jnp.bfloat16)
         back = [shift(summed[k], -k) if k else summed[0] for k in range(outer)]
-        turned = lax.dynamic_slice_in_dim(jnp.stack(back + back), outer - outer_index, outer, 0)
-        ffn_sum = jnp.transpose(turned, (1, 0, 2)).reshape(share, outer, inner, block)
-        ffn_sum = own_first(ffn_sum, inner_index, 2).reshape(share, width).astype(jnp.float32)
+        back = jnp.concatenate(back + back, axis=1)
+        ffn_sum = lax.dynamic_slice_in_dim(back, (outer - outer_index) * span, width, 1)
+        ffn_sum = own_first(ffn_sum, inner_index).astype(jnp.float32)
         return (middle.astype(jnp.float32) + ffn_sum).astype(jnp.bfloat16)
 
     return body
@@ -201,8 +232,10 @@
         P("sp", "tp"),
         P("tp", "sp"),
     )
+    body = make_body(mesh.shape["sp"], mesh.shape["tp"])
+
     return jax.shard_map(
-        make_body(mesh.shape["sp"], mesh.shape["tp"]),
+        body,
         mesh=mesh,
         in_specs=placed,
         out_specs=P(("sp", "tp"), None),

time: 522 us -> 459 us (0.88); the launches traced: 522 us -> 451 us
  waiting for transfers between devices: 393 us -> 260 us
  matrix products: 55.9 us -> 102 us
  starting transfers between devices: 23.2 us -> 58.7 us
  between operations: 13.7 us -> 1.31 us
  local copies, waits for them, and re-layouts: 16.4 us -> 6.59 us
    reduce_scatter x2 -> x0, waiting for transfers between devices: 75.2 us -> none  [the longest x1 45.6 us: body(): lax.psum_scatter(jnp.stack(terms), 'tp', scatter_dimension=1, tiled=True)]
    dot_general x3, matrix products: 11.8 us -> 74 us  [body(): part = jnp.dot(rows[k], gate_up, preferred_element_type=jnp.float32)]
    ppermute x0 -> x15, waiting for transfers between devices: none -> 61.9 us  [the longest x8 57.4 us: across(): return lax.ppermute(value, 'tp', [(t, t ^ step) for t in range(n_tp)])]
    all_gather x2 -> x0, waiting for transfers between devices: 59.7 us -> none  [the longest x1 59.7 us: body(): lax.all_gather(lax.dynamic_slice_in_dim(both, own_row, share, 0), ('sp',...]
    ppermute x12, waiting for transfers between devices: 189 us -> 144 us  [shift(): return lax.ppermute(value, 'sp', perm)]
    ppermute x0 -> x15, starting transfers between devices: none -> 18.4 us  [the longest x7 13.8 us: body(): lax.ppermute(both, 'sp', [(s, (s + k) % n_sp) for s in range(n_sp)])]
    ppermute x12, starting transfers between devices: 19.2 us -> 35.2 us  [shift(): return lax.ppermute(value, 'sp', perm)]
    ppermute x3, waiting for transfers between devices: 68.2 us -> 54.6 us  [with_partner(): return jnp.concatenate([value, lax.ppermute(value, 'sp', perm)], axis=axis)]
  transfers between devices with their start and end apart: 19 -> 30, of which waited for: 13 -> 20; matrix products, arithmetic and copies ran while one was open for 5% -> 13% of each run, Pallas kernels for 0% -> 0%
where the time goes in v2:
time: 459 us; the launch traced here: 451 us
  waiting for transfers between devices  260 us (57%)
  matrix products  102 us (22%)
  starting transfers between devices  58.7 us (13%)
  other arithmetic  15.3 us (3%)
  blocking collectives  7.08 us (2%)
  local copies, waits for them, and re-layouts  6.59 us (1%)
    ppermute x12, waiting for transfers between devices, shift(): return lax.ppermute(value, 'sp', perm)  144 us
    dot_general x3, matrix products, body(): part = jnp.dot(rows[k], gate_up, preferred_element_type=jnp.float32)  74 us
    ppermute x8, waiting for transfers between devices, across(): return lax.ppermute(value, 'tp', [(t, t ^ step) for t in range(n_tp)])  57.4 us
    ppermute x3, waiting for transfers between devices, with_partner(): return jnp.concatenate([value, lax.ppermute(value, 'sp', perm)], axis=axis)  54.6 us
    ppermute x12, starting transfers between devices, shift(): return lax.ppermute(value, 'sp', perm)  35.2 us
    ppermute x7, starting transfers between devices, body(): lax.ppermute(both, 'sp', [(s, (s + k) % n_sp) for s in range(n_sp)])  13.8 us
  transfers between devices with their start and end apart: 30, of which 20 were waited for; matrix products, arithmetic and copies ran while one was open for 13% of the time, Pallas kernels for 0%

profile of v2, /device:TPU:0, one launch (start us, length us, event | category | flops | bytes accessed | tf_op | source)
XLA Modules:
  0.0 451.0 jit_solution(13448069594234707993)
XLA Ops:
  0.0 1.0 copy.24
  1.0 0.9 bitcast_dynamic-update-slice_fusion.7
  1.9 3.0 collective-permute-start
  4.9 1.6 collective-permute-start.1
  6.5 2.6 collective-permute-start.2
  9.0 1.2 collective-permute-start.3
  10.2 2.6 collective-permute-start.4
  12.9 1.3 collective-permute-start.5
  14.2 1.5 collective-permute-start.6
  15.7 1.8 collective-permute-done.2
  17.6 0.7 collective-permute-done.3
  18.4 1.9 collective-permute-done.5
  20.3 1.6 collective-permute-start.7
  22.7 12.5 %collective-permute-done.7 = bf16[8,64,576]{2,1,0:T(8,128)(2,1)S(1)} collective-permute-done((bf16[8,64,576]{2,1,0:T(8,128)(2,1)S(1)}, bf16[8,64,576]{2,1,0:T(8,128)(2,1)S(1)}, u32[]{:S(2)}, u32[]{:S(2)}) %collective-permute-start.7) | collective-permute-done | bytes 589856 | tf_op jit(solution)/shard_map/ppermute | solution.py:72
  35.2 0.8 copy-done.4
  36.1 2.4 fusion.79
  39.0 0.7 subtract_convert_fusion
  39.7 1.1 broadcast_compare_fusion
  40.8 1.0 collective-permute-done.8
  41.8 1.7 pad_maximum_fusion
  44.4 2.6 convolution_convert_fusion.4
  47.0 2.0 copy-done.3
  49.0 4.6 %fusion.9 = f32[4,2048,256]{2,1,0:T(8,128)} fusion(bf16[2048,4,256]{0,2,1:T(8,128)(2,1)S(1)} %bitcast.162, bf16[256,4,192]{0,2,1:T(8,128)(2,1)S(1)} %bitcast.160), kind=kOutput, calls=%fused_computation.20 | convolution fusion | flops 536870912 | bytes 10747904 | tf_op jit(solution)/shard_map/qhd,khd->hqk/dot_general | solution.py:145
  53.8 1.2 fusion.53
  55.0 8.0 %fusion.85 = (f32[4,256]{1,0:T(4,128)S(1)}, bf16[4,256,2048]{1,2,0:T(8,128)(2,1)}) fusion(pred[256,2048]{0,1:T(8,128)(4,1)S(1)} %broadcast_compare_fusion, f32[4,2048,256]{2,1,0:T(8,128)} %fusion.9, bf16[2048,32]{0,1:T(8,128)(2,1)S(1)} %get-tuple-element.20, bf16[2048,32]{0,1:T(8,128)(2,1)S(1)} %get-tuple-element.19, ...), kind=kOutput, calls=%fused_computation.172 | convolution fusion | flops 283904000 | bytes 13504512 | tf_op jit(solution)/shard_map/sub | solution.py:155
  63.0 3.6 multiply_reduce_fusion
  67.0 7.1 %psum.7 = f32[256]{0:T(256)S(1)} all-reduce(f32[256]{0:T(256)S(1)} %get-tuple-element.40), channel_id=1, replica_groups=mesh['sp'=8,'tp'=4] {'tp'}, use_global_device_ids=true, to_apply=%region_4.5 | all-reduce | flops 256 | bytes 2048 | tf_op jit(solution)/shard_map/psum | solution.py:165
  74.3 3.4 convolution_convert_fusion
  78.0 2.6 collective-permute-done.9
  81.5 13.5 %collective-permute-done.10 = bf16[1,64,4096]{2,1,0:T(8,128)(2,1)S(1)} collective-permute-done((bf16[1,64,4096]{2,1,0:T(8,128)(2,1)S(1)}, bf16[1,64,4096]{2,1,0:T(8,128)(2,1)S(1)}, u32[]{:S(2)}, u32[]{:S(2)}) %collective-permute-start.10) | collective-permute-done | bytes 524320 | tf_op jit(solution)/shard_map/ppermute | solution.py:72
  94.9 1.4 fusion.38
  97.0 3.9 collective-permute-start.11
  100.9 0.9 collective-permute-start.12
  101.7 2.8 collective-permute-start.13
  104.8 5.1 %collective-permute-done.12 = bf16[64,1024]{1,0:T(8,128)(2,1)S(1)} collective-permute-done((bf16[64,1024]{1,0:T(8,128)(2,1)S(1)}, bf16[64,1024]{1,0:T(8,128)(2,1)S(1)}, u32[]{:S(2)}, u32[]{:S(2)}) %collective-permute-start.12) | collective-permute-done | bytes 131104 | tf_op jit(solution)/shard_map/ppermute | solution.py:56
  110.5 3.2 collective-permute-start.16
  113.8 10.0 %collective-permute-done.14 = bf16[4,64,1024]{2,1,0:T(8,128)(2,1)S(1)} collective-permute-done((bf16[4,64,1024]{2,1,0:T(8,128)(2,1)S(1)}, bf16[4,64,1024]{2,1,0:T(8,128)(2,1)S(1)}, u32[]{:S(2)}, u32[]{:S(2)}) %collective-permute-start.14) | collective-permute-done | bytes 524320 | tf_op jit(solution)/shard_map/ppermute | solution.py:72
  124.0 2.6 collective-permute-done.15
  127.0 21.9 %collective-permute-done.16 = bf16[512,1536]{1,0:T(8,128)(2,1)S(1)} collective-permute-done((bf16[512,1536]{1,0:T(8,128)(2,1)S(1)}, bf16[512,1536]{1,0:T(8,128)(2,1)S(1)}, u32[]{:S(2)}, u32[]{:S(2)}) %collective-permute-start.16) | collective-permute-done | bytes 1572896 | tf_op jit(solution)/shard_map/ppermute | solution.py:62
  148.9 32.7 %collective-permute-done.17 = bf16[512,1536]{1,0:T(8,128)(2,1)S(1)} collective-permute-done((bf16[512,1536]{1,0:T(8,128)(2,1)S(1)}, bf16[512,1536]{1,0:T(8,128)(2,1)S(1)}, u32[]{:S(2)}, u32[]{:S(2)}) %collective-permute-start.17) | collective-permute-done | bytes 1572896 | tf_op jit(solution)/shard_map/ppermute | solution.py:62
  181.6 24.6 %convolution_convert_fusion.3 = bf16[256,3072]{1,0:T(8,128)(2,1)S(1)} fusion(bf16[256,1024]{1,0:T(8,128)(2,1)S(1)} %bitcast.173, bf16[512,1536]{1,0:T(8,128)(2,1)S(1)} %collective-permute-done.17, bf16[512,1536]{1,0:T(8,128)(2,1)S(1)} %copy-done.12, bf16[512,1536]{1,0:T(8,128)(2,1)S(1)} %collective-permute-done.16, bf16[512,1536]{1,0:T(8,128)(2,1)S(1)} %copy-done.13), kind=kOutput, calls=%fused_computation.16 | convolution fusion | flops 1636564992 | bytes 8388608 | tf_op jit(solution)/shard_map/dot_general | solution.py:195
  206.2 3.6 collective-permute-start.18
  209.8 24.6 %convolution_convert_fusion.2 = bf16[256,3072]{1,0:T(8,128)(2,1)S(1)} fusion(bf16[256,1024]{1,0:T(8,128)(2,1)S(1)} %bitcast.171, bf16[512,1536]{1,0:T(8,128)(2,1)S(1)} %collective-permute-done.17, bf16[512,1536]{1,0:T(8,128)(2,1)S(1)} %copy-done.12, bf16[512,1536]{1,0:T(8,128)(2,1)S(1)} %collective-permute-done.16, bf16[512,1536]{1,0:T(8,128)(2,1)S(1)} %copy-done.13), kind=kOutput, calls=%fused_computation.15 | convolution fusion | flops 1636564992 | bytes 8388608 | tf_op jit(solution)/shard_map/dot_general | solution.py:195
  234.4 1.6 collective-permute-start.19
  235.9 24.8 %convolution_convert_fusion.1 = bf16[256,3072]{1,0:T(8,128)(2,1)S(1)} fusion(bf16[256,1024]{1,0:T(8,128)(2,1)S(1)} %bitcast.169, bf16[512,1536]{1,0:T(8,128)(2,1)S(1)} %collective-permute-done.17, bf16[512,1536]{1,0:T(8,128)(2,1)S(1)} %copy-done.12, bf16[512,1536]{1,0:T(8,128)(2,1)S(1)} %collective-permute-done.16, bf16[512,1536]{1,0:T(8,128)(2,1)S(1)} %copy-done.13), kind=kOutput, calls=%fused_computation.14 | convolution fusion | flops 1636564992 | bytes 8388608 | tf_op jit(solution)/shard_map/dot_general | solution.py:195
  260.9 1.8 collective-permute-start.21
  262.7 1.8 fusion.80
  264.5 81.3 %collective-permute-done.19 = bf16[256,3072]{1,0:T(8,128)(2,1)S(1)} collective-permute-done((bf16[256,3072]{1,0:T(8,128)(2,1)S(1)}, bf16[256,3072]{1,0:T(8,128)(2,1)S(1)}, u32[]{:S(2)}, u32[]{:S(2)}) %collective-permute-start.19) | collective-permute-done | bytes 1572896 | tf_op jit(solution)/shard_map/ppermute | solution.py:56
  345.8 0.9 convert_add_fusion
  347.8 4.2 collective-permute-start.24
  351.9 1.0 convolution_convert_fusion.8
  353.0 16.6 %collective-permute-done.22 = bf16[256,1536]{1,0:T(8,128)(2,1)S(1)} collective-permute-done((bf16[256,1536]{1,0:T(8,128)(2,1)S(1)}, bf16[256,1536]{1,0:T(8,128)(2,1)S(1)}, u32[]{:S(2)}, u32[]{:S(2)}) %collective-permute-start.22) | collective-permute-done | bytes 786464 | tf_op jit(solution)/shard_map/ppermute | solution.py:56
  369.5 1.0 convolution_convert_fusion.7
  370.6 30.0 %collective-permute-done.23 = bf16[256,1536]{1,0:T(8,128)(2,1)S(1)} collective-permute-done((bf16[256,1536]{1,0:T(8,128)(2,1)S(1)}, bf16[256,1536]{1,0:T(8,128)(2,1)S(1)}, u32[]{:S(2)}, u32[]{:S(2)}) %collective-permute-start.23) | collective-permute-done | bytes 786464 | tf_op jit(solution)/shard_map/ppermute | solution.py:56
  400.6 1.0 convolution_convert_fusion.6
  401.7 1.0 convolution_convert_fusion.5
  403.3 2.6 collective-permute-done.25
  406.4 1.6 collective-permute-start.26
  408.0 12.4 %collective-permute-done.26 = bf16[1,4,64,1024]{3,2,1,0:T(8,128)(2,1)S(1)} collective-permute-done((bf16[1,4,64,1024]{3,2,1,0:T(8,128)(2,1)S(1)}, bf16[1,4,64,1024]{3,2,1,0:T(8,128)(2,1)S(1)}, u32[]{:S(2)}, u32[]{:S(2)}) %collective-permute-start.26) | collective-permute-done | bytes 524320 | tf_op jit(solution)/shard_map/ppermute | solution.py:72
  420.7 17.5 %collective-permute-start.27 = (bf16[64,1024]{1,0:T(8,128)(2,1)S(1)}, bf16[64,1024]{1,0:T(8,128)(2,1)S(1)}, u32[]{:S(2)}, u32[]{:S(2)}) collective-permute-start(bf16[64,1024]{1,0:T(8,128)(2,1)S(1)} %get-tuple-element.23), channel_id=1, source_target_pairs={{0,24},{4,28},{8,0},{12,4},{16,8},{20,12},{24,16},{28,20},{1,25},{... | collective-permute-start | bytes 393224 | tf_op jit(solution)/shard_map/ppermute | solution.py:56
  438.2 0.7 collective-permute-start.29
  438.9 3.2 collective-permute-done.27
  442.1 7.1 %collective-permute-done.28 = bf16[64,1024]{1,0:T(8,128)(2,1)S(1)} collective-permute-done((bf16[64,1024]{1,0:T(8,128)(2,1)S(1)}, bf16[64,1024]{1,0:T(8,128)(2,1)S(1)}, u32[]{:S(2)}, u32[]{:S(2)}) %collective-permute-start.28) | collective-permute-done | bytes 131104 | tf_op jit(solution)/shard_map/ppermute | solution.py:56
  449.5 1.0 fusion.41
  (125 shorter events, 8.7 us)
Async XLA Ops:
  0.0 44.3 %copy-start = (bf16[512,1024]{1,0:T(8,128)(2,1)S(1)}, bf16[512,1024]{1,0:T(8,128)(2,1)}, u32[]{:S(2)}) copy-start(bf16[512,1024]{1,0:T(8,128)(2,1)} %param.17) | copy-start | bytes 3145732
  0.0 38.5 %copy-start.5 = (bf16[256,768]{1,0:T(8,128)(2,1)S(1)}, bf16[256,768]{1,0:T(8,128)(2,1)}, u32[]{:S(2)}) copy-start(bf16[256,768]{1,0:T(8,128)(2,1)} %param.13) | copy-start | bytes 1179652
  1.9 11.0 %collective-permute-start = (bf16[64,576]{1,0:T(8,128)(2,1)S(1)}, bf16[64,576]{1,0:T(8,128)(2,1)S(1)}, u32[]{:S(2)}, u32[]{:S(2)}) collective-permute-start(bf16[64,576]{1,0:T(8,128)(2,1)S(1)} %get-tuple-element.8), channel_id=1, source_target_pairs={{0,4},{4,8},{8,12},{12,16},{16,20},{20,24},{24,28},{28,0},{1,5},{5... | collective-permute-start | bytes 221192 | tf_op jit(solution)/shard_map/ppermute | solution.py:119
  4.9 9.4 %collective-permute-start.1 = (bf16[64,576]{1,0:T(8,128)(2,1)S(1)}, bf16[64,576]{1,0:T(8,128)(2,1)S(1)}, u32[]{:S(2)}, u32[]{:S(2)}) collective-permute-start(bf16[64,576]{1,0:T(8,128)(2,1)S(1)} %get-tuple-element.8), channel_id=1, source_target_pairs={{0,8},{4,12},{8,16},{12,20},{16,24},{20,28},{24,0},{28,4},{1,9},{5... | collective-permute-start | bytes 221192 | tf_op jit(solution)/shard_map/ppermute | solution.py:119
  6.5 11.1 %collective-permute-start.2 = (bf16[64,576]{1,0:T(8,128)(2,1)S(1)}, bf16[64,576]{1,0:T(8,128)(2,1)S(1)}, u32[]{:S(2)}, u32[]{:S(2)}) collective-permute-start(bf16[64,576]{1,0:T(8,128)(2,1)S(1)} %get-tuple-element.8), channel_id=1, source_target_pairs={{0,12},{4,16},{8,20},{12,24},{16,28},{20,0},{24,4},{28,8},{1,13},{... | collective-permute-start | bytes 221192 | tf_op jit(solution)/shard_map/ppermute | solution.py:119
  9.0 9.3 %collective-permute-start.3 = (bf16[64,576]{1,0:T(8,128)(2,1)S(1)}, bf16[64,576]{1,0:T(8,128)(2,1)S(1)}, u32[]{:S(2)}, u32[]{:S(2)}) collective-permute-start(bf16[64,576]{1,0:T(8,128)(2,1)S(1)} %get-tuple-element.8), channel_id=1, source_target_pairs={{0,16},{4,20},{8,24},{12,28},{16,0},{20,4},{24,8},{28,12},{1,17},{... | collective-permute-start | bytes 221192 | tf_op jit(solution)/shard_map/ppermute | solution.py:119
  10.2 8.1 %collective-permute-start.4 = (bf16[64,576]{1,0:T(8,128)(2,1)S(1)}, bf16[64,576]{1,0:T(8,128)(2,1)S(1)}, u32[]{:S(2)}, u32[]{:S(2)}) collective-permute-start(bf16[64,576]{1,0:T(8,128)(2,1)S(1)} %get-tuple-element.8), channel_id=1, source_target_pairs={{0,20},{4,24},{8,28},{12,0},{16,4},{20,8},{24,12},{28,16},{1,21},{... | collective-permute-start | bytes 221192 | tf_op jit(solution)/shard_map/ppermute | solution.py:119
  12.9 7.4 %collective-permute-start.5 = (bf16[64,576]{1,0:T(8,128)(2,1)S(1)}, bf16[64,576]{1,0:T(8,128)(2,1)S(1)}, u32[]{:S(2)}, u32[]{:S(2)}) collective-permute-start(bf16[64,576]{1,0:T(8,128)(2,1)S(1)} %get-tuple-element.8), channel_id=1, source_target_pairs={{0,24},{4,28},{8,0},{12,4},{16,8},{20,12},{24,16},{28,20},{1,25},{... | collective-permute-start | bytes 221192 | tf_op jit(solution)/shard_map/ppermute | solution.py:119
  14.2 6.1 %collective-permute-start.6 = (bf16[64,576]{1,0:T(8,128)(2,1)S(1)}, bf16[64,576]{1,0:T(8,128)(2,1)S(1)}, u32[]{:S(2)}, u32[]{:S(2)}) collective-permute-start(bf16[64,576]{1,0:T(8,128)(2,1)S(1)} %get-tuple-element.8), channel_id=1, source_target_pairs={{0,28},{4,0},{8,4},{12,8},{16,12},{20,16},{24,20},{28,24},{1,29},{... | collective-permute-start | bytes 221192 | tf_op jit(solution)/shard_map/ppermute | solution.py:119
  20.3 14.9 %collective-permute-start.7 = (bf16[8,64,576]{2,1,0:T(8,128)(2,1)S(1)}, bf16[8,64,576]{2,1,0:T(8,128)(2,1)S(1)}, u32[]{:S(2)}, u32[]{:S(2)}) collective-permute-start(bf16[8,64,576]{2,1,0:T(8,128)(2,1)S(1)} %bitcast_dynamic-update-slice_fusion), channel_id=1, source_target_pairs={{0,2},{1,3},{2,0},{3,1},{4,6},{5,7},{6,4},{7,5},{8,10},{9,11},{10,... | collective-permute-start | bytes 1769480 | tf_op jit(solution)/shard_map/ppermute | solution.py:72
  35.2 0.8 copy-start.4
  38.5 3.4 collective-permute-start.8
  38.5 1.2 copy-start.10
  43.6 0.8 copy-start.14
  46.9 2.0 copy-start.3
  49.0 4.9 %copy-start.11 = (f32[32]{0:T(128)S(1)}, f32[32]{0:T(128)}, u32[]{:S(2)}) copy-start(f32[32]{0:T(128)} %copy-done.10) | copy-start | bytes 388
  49.0 6.0 %copy-start.7 = (bf16[256,4,32]{0,2,1:T(8,128)(2,1)S(1)}, bf16[256,4,32]{0,2,1:T(8,128)(2,1)}, u32[]{:S(2)}) copy-start(bf16[256,4,32]{0,2,1:T(8,128)(2,1)} %get-tuple-element.30) | copy-start | bytes 196612
  49.0 6.0 %copy-start.8 = (bf16[256,4,32]{0,2,1:T(8,128)(2,1)S(1)}, bf16[256,4,32]{0,2,1:T(8,128)(2,1)}, u32[]{:S(2)}) copy-start(bf16[256,4,32]{0,2,1:T(8,128)(2,1)} %get-tuple-element.31) | copy-start | bytes 196612
  63.0 11.2 %copy-start.9 = (f32[512]{0:T(512)S(1)}, f32[512]{0:T(512)}, u32[]{:S(2)}) copy-start(f32[512]{0:T(512)} %param.18) | copy-start | bytes 6148
  77.9 18.5 %copy-start.6 = (f32[4096]{0:T(1024)S(1)}, f32[4096]{0:T(1024)}, u32[]{:S(2)}) copy-start(f32[4096]{0:T(1024)} %param.20) | copy-start | bytes 49156
  77.9 2.7 collective-permute-start.9
  80.9 14.0 %collective-permute-start.10 = (bf16[1,64,4096]{2,1,0:T(8,128)(2,1)S(1)}, bf16[1,64,4096]{2,1,0:T(8,128)(2,1)S(1)}, u32[]{:S(2)}, u32[]{:S(2)}) collective-permute-start(bf16[1,64,4096]{2,1,0:T(8,128)(2,1)S(1)} %slice_bitcast_fusion.4), channel_id=1, source_target_pairs={{0,2},{1,3},{2,0},{3,1},{4,6},{5,7},{6,4},{7,5},{8,10},{9,11},{10,... | collective-permute-start | bytes 1572872 | tf_op jit(solution)/shard_map/ppermute | solution.py:72
  96.4 14.1 %copy-start.13 = (bf16[512,1536]{1,0:T(8,128)(2,1)S(1)}, bf16[512,1536]{1,0:T(8,128)(2,1)}, u32[]{:S(2)}) copy-start(bf16[512,1536]{1,0:T(8,128)(2,1)} %param.21) | copy-start | bytes 4718596
  96.4 17.3 %copy-start.12 = (bf16[512,1536]{1,0:T(8,128)(2,1)S(1)}, bf16[512,1536]{1,0:T(8,128)(2,1)}, u32[]{:S(2)}) copy-start(bf16[512,1536]{1,0:T(8,128)(2,1)} %param.22) | copy-start | bytes 4718596
  97.0 7.8 %collective-permute-start.11 = (bf16[64,1024]{1,0:T(8,128)(2,1)S(1)}, bf16[64,1024]{1,0:T(8,128)(2,1)S(1)}, u32[]{:S(2)}, u32[]{:S(2)}) collective-permute-start(bf16[64,1024]{1,0:T(8,128)(2,1)S(1)} %get-tuple-element.29), channel_id=1, source_target_pairs={{0,8},{4,12},{8,16},{12,20},{16,24},{20,28},{24,0},{28,4},{1,9},{5... | collective-permute-start | bytes 393224 | tf_op jit(solution)/shard_map/ppermute | solution.py:56
  100.9 9.0 %collective-permute-start.12 = (bf16[64,1024]{1,0:T(8,128)(2,1)S(1)}, bf16[64,1024]{1,0:T(8,128)(2,1)S(1)}, u32[]{:S(2)}, u32[]{:S(2)}) collective-permute-start(bf16[64,1024]{1,0:T(8,128)(2,1)S(1)} %get-tuple-element.28), channel_id=1, source_target_pairs={{0,16},{4,20},{8,24},{12,28},{16,0},{20,4},{24,8},{28,12},{1,17},{... | collective-permute-start | bytes 393224 | tf_op jit(solution)/shard_map/ppermute | solution.py:56
  101.7 8.1 %collective-permute-start.13 = (bf16[64,1024]{1,0:T(8,128)(2,1)S(1)}, bf16[64,1024]{1,0:T(8,128)(2,1)S(1)}, u32[]{:S(2)}, u32[]{:S(2)}) collective-permute-start(bf16[64,1024]{1,0:T(8,128)(2,1)S(1)} %get-tuple-element.27), channel_id=1, source_target_pairs={{0,24},{4,28},{8,0},{12,4},{16,8},{20,12},{24,16},{28,20},{1,25},{... | collective-permute-start | bytes 393224 | tf_op jit(solution)/shard_map/ppermute | solution.py:56
  109.9 13.8 %collective-permute-start.14 = (bf16[4,64,1024]{2,1,0:T(8,128)(2,1)S(1)}, bf16[4,64,1024]{2,1,0:T(8,128)(2,1)S(1)}, u32[]{:S(2)}, u32[]{:S(2)}) collective-permute-start(bf16[4,64,1024]{2,1,0:T(8,128)(2,1)S(1)} %get-tuple-element.25), channel_id=1, source_target_pairs={{0,2},{1,3},{2,0},{3,1},{4,6},{5,7},{6,4},{7,5},{8,10},{9,11},{10,... | collective-permute-start | bytes 1572872 | tf_op jit(solution)/shard_map/ppermute | solution.py:72
  110.5 38.4 %collective-permute-start.16 = (bf16[512,1536]{1,0:T(8,128)(2,1)S(1)}, bf16[512,1536]{1,0:T(8,128)(2,1)S(1)}, u32[]{:S(2)}, u32[]{:S(2)}) collective-permute-start(bf16[512,1536]{1,0:T(8,128)(2,1)S(1)} %copy-done.13), channel_id=1, source_target_pairs={{0,4},{4,0},{8,12},{12,8},{16,20},{20,16},{24,28},{28,24},{1,5},{5... | collective-permute-start | bytes 4718600 | tf_op jit(solution)/shard_map/ppermute | solution.py:62
  113.7 67.9 %collective-permute-start.17 = (bf16[512,1536]{1,0:T(8,128)(2,1)S(1)}, bf16[512,1536]{1,0:T(8,128)(2,1)S(1)}, u32[]{:S(2)}, u32[]{:S(2)}) collective-permute-start(bf16[512,1536]{1,0:T(8,128)(2,1)S(1)} %copy-done.12), channel_id=1, source_target_pairs={{0,4},{4,0},{8,12},{12,8},{16,20},{20,16},{24,28},{28,24},{1,5},{5... | collective-permute-start | bytes 4718600 | tf_op jit(solution)/shard_map/ppermute | solution.py:62
  123.9 2.7 collective-permute-start.15
  206.2 58.3 %collective-permute-start.18 = (bf16[256,3072]{1,0:T(8,128)(2,1)S(1)}, bf16[256,3072]{1,0:T(8,128)(2,1)S(1)}, u32[]{:S(2)}, u32[]{:S(2)}) collective-permute-start(bf16[256,3072]{1,0:T(8,128)(2,1)S(1)} %convolution_convert_fusion.3), channel_id=1, source_target_pairs={{0,24},{4,28},{8,0},{12,4},{16,8},{20,12},{24,16},{28,20},{1,25},{... | collective-permute-start | bytes 4718600 | tf_op jit(solution)/shard_map/ppermute | solution.py:56
  234.4 111.5 %collective-permute-start.19 = (bf16[256,3072]{1,0:T(8,128)(2,1)S(1)}, bf16[256,3072]{1,0:T(8,128)(2,1)S(1)}, u32[]{:S(2)}, u32[]{:S(2)}) collective-permute-start(bf16[256,3072]{1,0:T(8,128)(2,1)S(1)} %convolution_convert_fusion.2), channel_id=1, source_target_pairs={{0,16},{4,20},{8,24},{12,28},{16,0},{20,4},{24,8},{28,12},{1,17},{... | collective-permute-start | bytes 4718600 | tf_op jit(solution)/shard_map/ppermute | solution.py:56
  235.9 24.9 %copy-start.2 = (bf16[1536,512]{1,0:T(8,128)(2,1)S(1)}, bf16[1536,512]{1,0:T(8,128)(2,1)}, u32[]{:S(2)}) copy-start(bf16[1536,512]{1,0:T(8,128)(2,1)} %param.23) | copy-start | bytes 4718596
  260.8 85.0 %collective-permute-start.20 = (bf16[256,3072]{1,0:T(8,128)(2,1)S(1)}, bf16[256,3072]{1,0:T(8,128)(2,1)S(1)}, u32[]{:S(2)}, u32[]{:S(2)}) collective-permute-start(bf16[256,3072]{1,0:T(8,128)(2,1)S(1)} %convolution_convert_fusion.1), channel_id=1, source_target_pairs={{0,8},{4,12},{8,16},{12,20},{16,24},{20,28},{24,0},{28,4},{1,9},{5... | collective-permute-start | bytes 4718600 | tf_op jit(solution)/shard_map/ppermute | solution.py:56
  260.9 86.7 %collective-permute-start.21 = (bf16[1536,512]{1,0:T(8,128)(2,1)S(1)}, bf16[1536,512]{1,0:T(8,128)(2,1)S(1)}, u32[]{:S(2)}, u32[]{:S(2)}) collective-permute-start(bf16[1536,512]{1,0:T(8,128)(2,1)S(1)} %copy-done.2), channel_id=1, source_target_pairs={{0,4},{4,0},{8,12},{12,8},{16,20},{20,16},{24,28},{28,24},{1,5},{5... | collective-permute-start | bytes 4718600 | tf_op jit(solution)/shard_map/ppermute | solution.py:62
  347.2 22.4 %collective-permute-start.22 = (bf16[256,1536]{1,0:T(8,128)(2,1)S(1)}, bf16[256,1536]{1,0:T(8,128)(2,1)S(1)}, u32[]{:S(2)}, u32[]{:S(2)}) collective-permute-start(bf16[256,1536]{1,0:T(8,128)(2,1)S(1)} %fusion.17), channel_id=1, source_target_pairs={{0,8},{4,12},{8,16},{12,20},{16,24},{20,28},{24,0},{28,4},{1,9},{5... | collective-permute-start | bytes 2359304 | tf_op jit(solution)/shard_map/ppermute | solution.py:56
  347.5 53.1 %collective-permute-start.23 = (bf16[256,1536]{1,0:T(8,128)(2,1)S(1)}, bf16[256,1536]{1,0:T(8,128)(2,1)S(1)}, u32[]{:S(2)}, u32[]{:S(2)}) collective-permute-start(bf16[256,1536]{1,0:T(8,128)(2,1)S(1)} %fusion.17), channel_id=1, source_target_pairs={{0,16},{4,20},{8,24},{12,28},{16,0},{20,4},{24,8},{28,12},{1,17},{... | collective-permute-start | bytes 2359304 | tf_op jit(solution)/shard_map/ppermute | solution.py:56
  347.8 53.9 %collective-permute-start.24 = (bf16[256,1536]{1,0:T(8,128)(2,1)S(1)}, bf16[256,1536]{1,0:T(8,128)(2,1)S(1)}, u32[]{:S(2)}, u32[]{:S(2)}) collective-permute-start(bf16[256,1536]{1,0:T(8,128)(2,1)S(1)} %fusion.17), channel_id=1, source_target_pairs={{0,24},{4,28},{8,0},{12,4},{16,8},{20,12},{24,16},{28,20},{1,25},{... | collective-permute-start | bytes 2359304 | tf_op jit(solution)/shard_map/ppermute | solution.py:56
  403.2 2.7 collective-permute-start.25
  406.4 14.0 %collective-permute-start.26 = (bf16[1,4,64,1024]{3,2,1,0:T(8,128)(2,1)S(1)}, bf16[1,4,64,1024]{3,2,1,0:T(8,128)(2,1)S(1)}, u32[]{:S(2)}, u32[]{:S(2)}) collective-permute-start(bf16[1,4,64,1024]{3,2,1,0:T(8,128)(2,1)S(1)} %slice_bitcast_fusion.2), channel_id=1, source_target_pairs={{0,2},{1,3},{2,0},{3,1},{4,6},{5,7},{6,4},{7,5},{8,10},{9,11},{10,... | collective-permute-start | bytes 1572872 | tf_op jit(solution)/shard_map/ppermute | solution.py:72
  420.4 30.1 %copy-start.1 = (bf16[512,1024]{1,0:T(8,128)(2,1)S(1)}, bf16[512,1024]{1,0:T(8,128)(2,1)}, u32[]{:S(2)}) copy-start(bf16[512,1024]{1,0:T(8,128)(2,1)} %param.17) | copy-start | bytes 3145732
  420.7 21.4 %collective-permute-start.27 = (bf16[64,1024]{1,0:T(8,128)(2,1)S(1)}, bf16[64,1024]{1,0:T(8,128)(2,1)S(1)}, u32[]{:S(2)}, u32[]{:S(2)}) collective-permute-start(bf16[64,1024]{1,0:T(8,128)(2,1)S(1)} %get-tuple-element.23), channel_id=1, source_target_pairs={{0,24},{4,28},{8,0},{12,4},{16,8},{20,12},{24,16},{28,20},{1,25},{... | collective-permute-start | bytes 393224 | tf_op jit(solution)/shard_map/ppermute | solution.py:56
  438.2 11.0 %collective-permute-start.28 = (bf16[64,1024]{1,0:T(8,128)(2,1)S(1)}, bf16[64,1024]{1,0:T(8,128)(2,1)S(1)}, u32[]{:S(2)}, u32[]{:S(2)}) collective-permute-start(bf16[64,1024]{1,0:T(8,128)(2,1)S(1)} %get-tuple-element.22), channel_id=1, source_target_pairs={{0,16},{4,20},{8,24},{12,28},{16,0},{20,4},{24,8},{28,12},{1,17},{... | collective-permute-start | bytes 393224 | tf_op jit(solution)/shard_map/ppermute | solution.py:56
  438.2 11.0 %collective-permute-start.29 = (bf16[64,1024]{1,0:T(8,128)(2,1)S(1)}, bf16[64,1024]{1,0:T(8,128)(2,1)S(1)}, u32[]{:S(2)}, u32[]{:S(2)}) collective-permute-start(bf16[64,1024]{1,0:T(8,128)(2,1)S(1)} %get-tuple-element.21), channel_id=1, source_target_pairs={{0,8},{4,12},{8,16},{12,20},{16,24},{20,28},{24,0},{28,4},{1,9},{5... | collective-permute-start | bytes 393224 | tf_op jit(solution)/shard_map/ppermute | solution.py:56
